TPU v7x, 32 devices: a whole 2x2x4 slice. The times are simulated.
32 devices in a mesh: kv: 8 (over z, core), tp: 4 (over y, x).
Axes of the slice: x: 2, y: 2, z: 4, core: 2. Of those that a mesh axis runs over, the one named last changes fastest.
Arguments:
- tokens: bfloat16 [128, 4096], P(None, 'kv'), may hold values from -40 to 40
- gain_first: float32 [4096], P('kv'), may hold values from 0.1 to 1.9
- gate_first: bfloat16 [4096, 11008], P('kv', 'tp'), may hold values from -0.09375 to 0.09375
- up_first: bfloat16 [4096, 11008], P('kv', 'tp'), may hold values from -0.09375 to 0.09375
- down_first: bfloat16 [11008, 4096], P('tp', 'kv'), may hold values from -0.0546875 to 0.0546875
- gain_mix: float32 [4096], P('kv'), may hold values from 0.1 to 1.9
- w_query: bfloat16 [4096, 2048], P('kv', 'tp'), may hold values from -0.09375 to 0.09375
- w_key: bfloat16 [4096, 2048], P('kv', 'tp'), may hold values from -0.09375 to 0.09375
- w_value: bfloat16 [4096, 2048], P('kv', 'tp'), may hold values from -0.09375 to 0.09375
- w_outgate: bfloat16 [4096, 2048], P('kv', 'tp'), may hold values from -0.09375 to 0.09375
- w_ingate: bfloat16 [4096, 16], P('kv'), may hold values from -0.046875 to 0.046875
- w_forget: bfloat16 [4096, 16], P('kv'), may hold values from -0.09375 to 0.09375
- forget_bias: float32 [16], P('tp'), may hold values from -1 to 4
- memory: float32 [128, 16, 128, 128], P('kv', 'tp'), may hold values from -0.6 to 0.6
- normalizer: float32 [128, 16, 128], P('kv', 'tp'), may hold values from -0.6 to 0.6
- stabilizer: float32 [128, 16], P('kv', 'tp'), may hold values from -3 to 0.5
- w_project: bfloat16 [2048, 4096], P('tp', 'kv'), may hold values from -0.75 to 0.75
- gain_second: float32 [4096], P('kv'), may hold values from 0.3 to 3
- gate_second: bfloat16 [4096, 11008], P('kv', 'tp'), may hold values from -0.09375 to 0.09375
- up_second: bfloat16 [4096, 11008], P('kv', 'tp'), may hold values from -0.09375 to 0.09375
- down_second: bfloat16 [11008, 4096], P('tp', 'kv'), may hold values from -0.0546875 to 0.0546875
Outputs:
- mixed_out: bfloat16 [128, 4096], P(None, 'kv')
- memory_new: float32 [128, 16, 128, 128], P('kv', 'tp')
- normalizer_new: float32 [128, 16, 128], P('kv', 'tp')
- stabilizer_new: float32 [128, 16], P('kv', 'tp')
All inputs are finite; a program needn't handle non-finite values.
Results may differ from a plain program's by a relative error of at most 0.04.
Values may be sent and summed in bfloat16 or wider, within the bound.
A program may use at most 64 MiB of HBM per device.

v0:
```python
import functools
from types import SimpleNamespace as NS

import jax
import jax.numpy as jnp
from jax import lax
from jax.experimental import pallas as pl
from jax.experimental.pallas import tpu as pltpu
from jax.sharding import PartitionSpec as P

EPSILON = 1e-06
LANES = 128
CHUNKS = 4
MESH = pl.DeviceIdType.MESH
BF = jnp.bfloat16
F32 = jnp.float32


def chunks_of(hidden):
    size = -(-hidden // (CHUNKS * 256)) * 256
    return [(at, min(size, hidden - at)) for at in range(0, hidden, size)]


def layer_kernel(n_kv, n_tp, unpack, *refs):
    arg, out, mem = unpack(refs)
    nz = n_kv // 2
    me = lax.axis_index("kv")
    z, c = me // 2, lax.rem(me, 2)
    tp = lax.axis_index("tp")
    partner = me + 1 - 2 * c
    rows, width = arg.tokens.shape
    d_model = width * n_kv
    rb = rows // n_kv
    rt = rows // n_tp
    head_size = arg.memory.shape[-1]
    heads = arg.memory.shape[1]

    loads = {}
    for i, (name, ref) in enumerate(mem.held.items()):
        loads[name] = pltpu.make_async_copy(getattr(arg, name), ref, mem.load_sem.at[i])
        loads[name].start()
    held = NS(**mem.held)
    load = NS(**loads)

    barrier = pltpu.get_barrier_semaphore()
    for d in range(1, n_kv):
        pl.semaphore_signal(barrier, inc=1, device_id={"kv": lax.rem(me + d, n_kv)}, device_id_type=MESH)
    for d in range(1, n_tp):
        pl.semaphore_signal(barrier, inc=1, device_id={"tp": lax.rem(tp + d, n_tp)}, device_id_type=MESH)
    pl.semaphore_wait(barrier, n_kv + n_tp - 2)

    pending = []

    def remote(src, dst, send_sem, recv_sem, where):
        return pltpu.make_async_remote_copy(
            src_ref=src, dst_ref=dst, send_sem=send_sem, recv_sem=recv_sem, device_id=where, device_id_type=MESH)

    def send(*args):
        copy = remote(*args)
        copy.start()
        pending.append(copy)

    def arrived(dst, send_sem, recv_sem):
        remote(dst, dst, send_sem, recv_sem, {"kv": partner}).wait_recv()

    def flat(ref):
        a, b, w = ref.shape
        return ref[...].reshape(a * b, w)

    def norm_prepare(n, x, gain):
        wide = x.astype(F32)
        mem.scaled[...] = (wide * gain[...]).astype(BF)
        part = jnp.sum(wide * wide, axis=1, keepdims=True)
        n.sq_out[...] = jnp.broadcast_to(part, (rows, LANES)).reshape(n_kv, rb, LANES)
        for d in range(1, n_kv):
            peer = lax.rem(me + d, n_kv)
            send(n.sq_out.at[peer], n.sq_in.at[d], n.sq_s.at[d], n.sq_r.at[d], {"kv": peer})

    def norm_scale(n):
        total = n.sq_out[me]
        for d in range(1, n_kv):
            arrived(n.sq_in.at[d], n.sq_s.at[d], n.sq_r.at[d])
            total = total + n.sq_in[d]
        return lax.rsqrt(total / d_model + EPSILON)[:, :1]

    def rows_dot(weight):
        return lax.dot_general(
            mem.scaled[...], weight, (((1,), (1,)), ((), ())), preferred_element_type=F32).astype(BF)

    def keep(buf, g, val, place):
        for i in range(n_kv):
            buf[i % 2, i // 2, g, :, place] = val[i * rb:(i + 1) * rb]

    def product(weight, start, size, buf, g):
        step = 256
        full = size // step

        def tile(off, n, place):
            keep(buf, g, rows_dot(weight[pl.ds(off, n), :]), pl.ds(place, n))

        if full:
            @pl.loop(0, full)
            def _(t):
                tile(pl.multiple_of(start + t * step, 16), step, pl.multiple_of(t * step, step))
        if size > full * step:
            tile(start + full * step, size - full * step, full * step)

    def scatter_pair(s):
        for d in range(nz):
            chip = lax.rem(z + d + 1, nz)
            send(s.a.at[1 - c, chip], s.b.at[chip], s.s1.at[d], s.r1.at[d], {"kv": partner})

    def scatter_chips(s):
        for d in range(nz):
            chip = lax.rem(z + d + 1, nz)
            arrived(s.b.at[chip], s.s1.at[d], s.r1.at[d])
            if d < nz - 1:
                s.c[d] = (s.a[c, chip].astype(F32) + s.b[chip].astype(F32)).astype(BF)
                send(s.c.at[d], s.d.at[d], s.s2.at[d], s.r2.at[d], {"kv": chip * 2 + c})

    def scatter_sum(s):
        total = s.a[c, z].astype(F32) + s.b[z].astype(F32)
        for d in range(nz - 1):
            arrived(s.d.at[d], s.s2.at[d], s.r2.at[d])
            total = total + s.d[d].astype(F32)
        return total

    def gather_start(s):
        for d in range(nz - 1):
            chip = lax.rem(z + d + 1, nz)
            send(s.g.at[me], s.g.at[me], s.gs.at[d], s.gr.at[d], {"kv": chip * 2 + c})
        send(s.g.at[me], s.g.at[me], s.hs.at[nz - 1], s.hr.at[nz - 1], {"kv": partner})

    def gather_forward(s):
        for d in range(nz - 1):
            block = lax.rem(z - d - 1 + nz, nz) * 2 + c
            arrived(s.g.at[block], s.gs.at[d], s.gr.at[d])
            send(s.g.at[block], s.g.at[block], s.hs.at[d], s.hr.at[d], {"kv": partner})

    def gather_wait(s):
        for d in range(nz):
            block = lax.rem(z - d - 1 + nz, nz) * 2 + 1 - c
            arrived(s.g.at[block], s.hs.at[d], s.hr.at[d])

    def sum_tp(n, acc, residual, factor):
        mem.acc[...] = acc
        for j in range(n_tp):
            n.p[j] = acc[j * rt:(j + 1) * rt].astype(BF)
        for d in range(1, n_tp):
            peer = lax.rem(tp + d, n_tp)
            send(n.p.at[peer], n.q.at[d], n.ps.at[d], n.pr.at[d], {"tp": peer})
        total = mem.acc[pl.ds(pl.multiple_of(tp * rt, rt), rt)]
        for d in range(1, n_tp):
            arrived(n.q.at[d], n.ps.at[d], n.pr.at[d])
            total = total + n.q[d].astype(F32)
        n.o[tp] = (residual.astype(F32) + factor * total).astype(BF)
        for d in range(1, n_tp):
            peer = lax.rem(tp + d, n_tp)
            send(n.o.at[tp], n.o.at[tp], n.os.at[d], n.ur.at[d], {"tp": peer})
        for d in range(1, n_tp):
            source = lax.rem(tp - d + n_tp, n_tp)
            arrived(n.o.at[source], n.os.at[d], n.ur.at[d])

    def half_step(n, x, residual, gain, gate, up, down, load_gate, load_up, load_down):
        norm_prepare(n, x, gain)
        pieces = list(zip(chunks_of(gate.shape[0]), n.parts))
        load_gate.wait()
        for i, ((start, size), s) in enumerate(pieces):
            product(gate, start, size, s.a, 0)
            if i == 0:
                load_up.wait()
            product(up, start, size, s.a, 1)
            scatter_pair(s)
            if i > 0:
                scatter_chips(pieces[i - 1][1])
        scatter_chips(pieces[-1][1])
        scale = norm_scale(n)
        for i, (_, s) in enumerate(pieces):
            total = scatter_sum(s)
            gate_values, up_values = scale * total[0], scale * total[1]
            s.g[me] = (gate_values / (1.0 + jnp.exp(-gate_values)) * up_values).astype(BF)
            gather_start(s)
            if i > 0:
                gather_forward(pieces[i - 1][1])
        gather_forward(pieces[-1][1])
        load_down.wait()
        acc = jnp.zeros((rows, width), F32)
        for (start, size), s in pieces:
            gather_wait(s)
            acc = acc + jnp.dot(flat(s.g), down[start:start + size, :], preferred_element_type=F32)
        sum_tp(n, acc, residual(), 0.5)

    own_tp = pl.ds(pl.multiple_of(tp * rt, rt), rt)
    half_step(mem.first, arg.tokens[...], lambda: arg.tokens[own_tp], arg.gain_first, held.gate_first,
              held.up_first, held.down_first, load.gate_first, load.up_first, load.down_first)

    n = mem.mix
    norm_prepare(n, flat(mem.first.o), arg.gain_mix)
    dm = arg.w_query.shape[1]
    n_heads = arg.w_ingate.shape[0]
    one, two = n.parts

    def wide_product(weight, s, at):
        val = jnp.dot(mem.scaled[...], weight[...], preferred_element_type=F32).astype(BF)
        keep(s.a, 0, val, slice(at, at + dm))

    load.w_query.wait()
    wide_product(held.w_query, one, 0)
    load.w_key.wait()
    wide_product(held.w_key, one, dm)
    gates = rows_dot(jnp.concatenate([arg.w_ingate[...], arg.w_forget[...]], axis=0))
    gates = jnp.concatenate([gates, jnp.zeros((rows, LANES - 2 * n_heads), BF)], axis=1)
    keep(one.a, 0, gates, slice(2 * dm, 2 * dm + LANES))
    scatter_pair(one)
    load.w_value.wait()
    wide_product(held.w_value, two, 0)
    load.w_outgate.wait()
    wide_product(held.w_outgate, two, dm)
    scatter_pair(two)
    scatter_chips(one)
    scatter_chips(two)
    scale = norm_scale(n)
    total = scale * scatter_sum(one)[0]
    total_two = scale * scatter_sum(two)[0]

    gates = total[:, 2 * dm:]
    lane = lax.broadcasted_iota(jnp.int32, (rb, LANES), 1)
    diagonal = lax.broadcasted_iota(jnp.int32, (rb, rb), 0) == lax.broadcasted_iota(jnp.int32, (rb, rb), 1)
    load.memory.wait()
    state = held.memory
    parts = []
    for h in range(heads):
        low, high = h * head_size, (h + 1) * head_size
        q, k, v, gate_out = (
            val.astype(BF).astype(F32)
            for val in (total[:, low:high], total[:, dm + low:dm + high],
                        total_two[:, low:high], total_two[:, dm + low:dm + high]))
        k = k * head_size ** (-0.5)
        ingate = jnp.sum(jnp.where(lane == tp * heads + h, gates, 0.0), axis=1, keepdims=True)
        forget = jnp.sum(jnp.where(lane == n_heads + tp * heads + h, gates, 0.0), axis=1, keepdims=True)
        forget = forget + arg.forget_bias[h]
        log_forget = jnp.minimum(forget, 0.0) - jnp.log1p(jnp.exp(-jnp.abs(forget)))
        stabilizer = jnp.sum(jnp.where(diagonal, arg.stabilizer[h:h + 1, :], 0.0), axis=1, keepdims=True)
        kept = log_forget + stabilizer
        ceiling = jnp.maximum(kept, ingate)
        fresh = jnp.exp(ingate - ceiling)
        carried = jnp.exp(kept - ceiling)
        out.stabilizer_new[h:h + 1, :] = jnp.sum(jnp.where(diagonal, ceiling, 0.0), axis=0, keepdims=True)
        norm = arg.normalizer[:, h, :]
        out.normalizer_new[:, h, :] = carried * norm + fresh * k
        own = jnp.sum(q * k, axis=1, keepdims=True) * fresh
        den = own + carried * jnp.sum(norm * q, axis=1, keepdims=True)
        den = jnp.maximum(jnp.abs(den), jnp.exp(-ceiling))
        mem.row_q[h] = q
        mem.row_k[h] = fresh * k
        mem.row_c[h] = jnp.broadcast_to(carried, (rb, head_size))
        pad = jnp.zeros((LANES - rb, head_size), F32)
        mem.col_v[h] = jnp.concatenate([v, pad], axis=0).T
        mem.col_r[h] = jnp.zeros((head_size, LANES), F32)
        parts.append((own, v, carried, den, gate_out))

    lane2 = lax.broadcasted_iota(jnp.int32, (head_size, LANES), 1)

    @pl.loop(0, rb)
    def _(b):
        for h in range(heads):
            recall = jnp.sum(state[b, h] * mem.row_q[h, pl.ds(b, 1), :], axis=1, keepdims=True)
            mem.col_r[h] = jnp.where(lane2 == b, recall, mem.col_r[h])

    for h in range(heads):
        own, v, carried, den, gate_out = parts[h]
        recall = mem.col_r[h].T[:rb]
        readout = (own * v + carried * recall) / den
        n.parts[0].g[me, :, h * head_size:(h + 1) * head_size] = (
            readout / (1.0 + jnp.exp(-gate_out))).astype(BF)
    gather_start(one)

    @pl.loop(0, rb)
    def _(b):
        for h in range(heads):
            v_col = jnp.sum(jnp.where(lane2 == b, mem.col_v[h], 0.0), axis=1, keepdims=True)
            state[b, h] = (mem.row_c[h, pl.ds(b, 1), :] * state[b, h]
                           + v_col * mem.row_k[h, pl.ds(b, 1), :])

    store = pltpu.make_async_copy(state, out.memory_new, mem.load_sem.at[len(mem.held)])
    store.start()
    gather_forward(one)
    load.w_project.wait()
    gather_wait(one)
    sum_tp(n, jnp.dot(flat(one.g), held.w_project[...], preferred_element_type=F32), mem.first.o[tp], 1.0)

    half_step(mem.second, flat(n.o), lambda: n.o[tp], arg.gain_second, held.gate_second,
              held.up_second, held.down_second, load.gate_second, load.up_second, load.down_second)
    out.mixed_out[...] = flat(mem.second.o)
    store.wait()
    for copy in pending:
        copy.wait_send()


def on_device(
    n_kv, n_tp, tokens, gain_first, gate_first, up_first, down_first, gain_mix, w_query, w_key, w_value,
    w_outgate, w_ingate, w_forget, forget_bias, memory, normalizer, stabilizer, w_project, gain_second,
    gate_second, up_second, down_second,
):
    rows, width = tokens.shape
    hidden = gate_first.shape[1]
    dm = w_query.shape[1]
    nz, rb, rt = n_kv // 2, rows // n_kv, rows // n_tp
    heads, head_size = memory.shape[1], memory.shape[3]
    dma = pltpu.SemaphoreType.DMA

    in_vmem = dict(
        tokens=tokens, gain_first=gain_first.reshape(1, -1), gain_mix=gain_mix.reshape(1, -1),
        gain_second=gain_second.reshape(1, -1), w_ingate=w_ingate.T, w_forget=w_forget.T,
        normalizer=normalizer, stabilizer=stabilizer.T)
    in_smem = dict(forget_bias=forget_bias)
    streamed = dict(
        gate_first=gate_first.T, up_first=up_first.T, down_first=down_first, w_query=w_query, w_key=w_key,
        w_value=w_value, w_outgate=w_outgate, memory=memory, w_project=w_project, gate_second=gate_second.T,
        up_second=up_second.T, down_second=down_second)
    operands = {**in_vmem, **in_smem, **streamed}
    results = dict(
        mixed_out=jax.ShapeDtypeStruct(tokens.shape, BF),
        memory_new=jax.ShapeDtypeStruct(memory.shape, F32),
        normalizer_new=jax.ShapeDtypeStruct(normalizer.shape, F32),
        stabilizer_new=jax.ShapeDtypeStruct(stabilizer.shape[::-1], F32))

    def exchange(g, cols, gathered):
        bufs = dict(
            a=pltpu.VMEM((2, nz, g, rb, cols), BF), b=pltpu.VMEM((nz, g, rb, cols), BF),
            c=pltpu.VMEM((nz, g, rb, cols), BF), d=pltpu.VMEM((nz, g, rb, cols), BF),
            s1=dma((nz,)), r1=dma((nz,)), s2=dma((nz,)), r2=dma((nz,)))
        if gathered:
            bufs.update(
                g=pltpu.VMEM((n_kv, rb, gathered), BF), gs=dma((nz,)), gr=dma((nz,)), hs=dma((nz,)), hr=dma((nz,)))
        return bufs

    def phase(parts):
        return dict(
            parts=parts,
            sq_out=pltpu.VMEM((n_kv, rb, LANES), F32), sq_in=pltpu.VMEM((n_kv, rb, LANES), F32),
            sq_s=dma((n_kv,)), sq_r=dma((n_kv,)),
            p=pltpu.VMEM((n_tp, rt, width), BF), q=pltpu.VMEM((n_tp, rt, width), BF),
            o=pltpu.VMEM((n_tp, rt, width), BF),
            ps=dma((n_tp,)), pr=dma((n_tp,)), os=dma((n_tp,)), ur=dma((n_tp,)))

    tree = dict(
        held={name: pltpu.VMEM(a.shape, a.dtype) for name, a in streamed.items()},
        load_sem=dma((len(streamed) + 1,)),
        scaled=pltpu.VMEM((rows, width), BF),
        acc=pltpu.VMEM((rows, width), F32),
        first=phase([exchange(2, size, size) for _, size in chunks_of(hidden)]),
        mix=phase([exchange(1, 2 * dm + LANES, dm), exchange(1, 2 * dm, 0)]),
        second=phase([exchange(2, size, size) for _, size in chunks_of(hidden)]),
        row_q=pltpu.VMEM((heads, rb, head_size), F32),
        row_k=pltpu.VMEM((heads, rb, head_size), F32),
        row_c=pltpu.VMEM((heads, rb, head_size), F32),
        col_v=pltpu.VMEM((heads, head_size, LANES), F32),
        col_r=pltpu.VMEM((heads, head_size, LANES), F32))

    shapes = []

    def number(node):
        if isinstance(node, dict):
            return {key: number(value) for key, value in node.items()}
        if isinstance(node, list):
            return [number(value) for value in node]
        shapes.append(node)
        return len(shapes) - 1

    numbered = number(tree)

    def unpack(refs):
        n_in, n_out = len(operands), len(results)
        scratch = refs[n_in + n_out:]

        def fill(node):
            if isinstance(node, dict):
                return NS(**{key: fill(value) for key, value in node.items()})
            if isinstance(node, list):
                return [fill(value) for value in node]
            return scratch[node]

        mem = fill(numbered)
        mem.held = {name: scratch[i] for name, i in numbered["held"].items()}
        return NS(**dict(zip(operands, refs))), NS(**dict(zip(results, refs[n_in:]))), mem

    vm = pl.BlockSpec(memory_space=pltpu.VMEM)
    hbm = pl.BlockSpec(memory_space=pl.ANY)
    mixed_out, memory_new, normalizer_new, stabilizer_new = pl.pallas_call(
        functools.partial(layer_kernel, n_kv, n_tp, unpack),
        out_shape=list(results.values()),
        in_specs=[vm] * len(in_vmem) + [pl.BlockSpec(memory_space=pltpu.SMEM)] + [hbm] * len(streamed),
        out_specs=[vm, hbm, vm, vm],
        scratch_shapes=shapes,
        compiler_params=pltpu.CompilerParams(
            collective_id=0, has_side_effects=True, vmem_limit_bytes=60 * 2**20),
    )(*operands.values())
    return mixed_out, memory_new, normalizer_new, stabilizer_new.T


def solution(mesh):
    kv, tp, both = P("kv"), P("tp"), P("kv", "tp")
    width, back = P(None, "kv"), P("tp", "kv")
    return jax.shard_map(
        functools.partial(on_device, mesh.shape["kv"], mesh.shape["tp"]),
        mesh=mesh,
        in_specs=(width, kv, both, both, back, kv, both, both, both, both, kv, kv, tp, both, both, both,
                  back, kv, both, both, back),
        out_specs=(width, both, both, both),
        check_vma=False,
    )
```

profile of v0, /device:TPU:0, one launch (start us, length us, event | category | flops | bytes accessed | tf_op | source)
XLA Modules:
  0.0 117.7 jit_solution(46749855879310529)
XLA Ops:
  0.6 109.6 %shard_map.228 = (bf16[128,512]{1,0:T(8,128)(2,1)}, f32[16,4,128,128]{3,2,1,0:T(8,128)}, f32[16,4,128]{2,1,0:T(4,128)}, f32[4,16]{1,0:T(4,128)}) custom-call(bf16[128,512]{1,0:T(8,128)(2,1)} %refs_0_.1, f32[1,512]{1,0:T(1,128)} %bitcast.17, f32[1,512]{1,0:T(1,128)} %bitcast.18, f32[1,512]{1,0:T(1,128)} %bitcast.19, bf16[16,512]{1,0:T(8,128)(2,1)} %bitcast.15, ...), custom_call_target="tpu_custom_call" | custom-call | tf_op jit(solution)/shard_map/pallas_call | solution.py:390
  110.2 1.6 %copy.29 = bf16[128,512]{1,0:T(8,128)(2,1)} copy(bf16[128,512]{1,0:T(8,128)(2,1)} %get-tuple-element.16) | data formatting | bytes 262144
  111.8 0.0 copy-start
  111.8 0.0 copy-start.1
  111.8 4.7 %copy.30 = f32[16,4,128,128]{3,2,1,0:T(8,128)} copy(f32[16,4,128,128]{3,2,1,0:T(8,128)} %get-tuple-element.17) | data formatting | bytes 8388608
  116.5 0.0 copy-done
  116.5 0.6 copy.31
  117.1 0.0 copy-done.1
  117.1 0.6 copy.32
Async XLA Ops:
  111.8 4.7 %copy-start = (f32[16,4,128]{2,1,0:T(4,128)S(1)}, f32[16,4,128]{2,1,0:T(4,128)}, u32[]{:S(2)}) copy-start(f32[16,4,128]{2,1,0:T(4,128)} %get-tuple-element.18) | copy-start | bytes 98308
  111.8 5.3 %copy-start.1 = (f32[4,16]{1,0:T(4,128)S(1)}, f32[4,16]{1,0:T(4,128)}, u32[]{:S(2)}) copy-start(f32[4,16]{1,0:T(4,128)} %get-tuple-element.11) | copy-start | bytes 772
where the time goes:
time: 118 us
  Pallas kernels  110 us (93%)
  local copies, waits for them, and re-layouts  7.47 us (6%)
    pallas_call x1, Pallas kernels, on_device(): pl.pallas_call(functools.partial(layer_kernel, n_kv, n_tp, unpack), out_s...  110 us
    unnamed x8, local copies, waits for them, and re-layouts  7.47 us

commit v1 on v0

--- a/solution.py
+++ b/solution.py
@@ -1,4 +1,5 @@
 import functools
+import math
 from types import SimpleNamespace as NS
 
 import jax
@@ -47,7 +48,9 @@
         pl.semaphore_signal(barrier, inc=1, device_id={"kv": lax.rem(me + d, n_kv)}, device_id_type=MESH)
     for d in range(1, n_tp):
         pl.semaphore_signal(barrier, inc=1, device_id={"tp": lax.rem(tp + d, n_tp)}, device_id_type=MESH)
-    pl.semaphore_wait(barrier, n_kv + n_tp - 2)
+
+    def everyone_here():
+        pl.semaphore_wait(barrier, n_kv + n_tp - 2)
 
     pending = []
 
@@ -72,6 +75,8 @@
         mem.scaled[...] = (wide * gain[...]).astype(BF)
         part = jnp.sum(wide * wide, axis=1, keepdims=True)
         n.sq_out[...] = jnp.broadcast_to(part, (rows, LANES)).reshape(n_kv, rb, LANES)
+
+    def norm_send(n):
         for d in range(1, n_kv):
             peer = lax.rem(me + d, n_kv)
             send(n.sq_out.at[peer], n.sq_in.at[d], n.sq_s.at[d], n.sq_r.at[d], {"kv": peer})
@@ -161,8 +166,10 @@
             source = lax.rem(tp - d + n_tp, n_tp)
             arrived(n.o.at[source], n.os.at[d], n.ur.at[d])
 
-    def half_step(n, x, residual, gain, gate, up, down, load_gate, load_up, load_down):
+    def half_step(n, x, residual, gain, gate, up, down, load_gate, load_up, load_down, ready=None):
         norm_prepare(n, x, gain)
+        if ready is None:
+            norm_send(n)
         pieces = list(zip(chunks_of(gate.shape[0]), n.parts))
         load_gate.wait()
         for i, ((start, size), s) in enumerate(pieces):
@@ -170,6 +177,9 @@
             if i == 0:
                 load_up.wait()
             product(up, start, size, s.a, 1)
+            if i == 0 and ready is not None:
+                ready()
+                norm_send(n)
             scatter_pair(s)
             if i > 0:
                 scatter_chips(pieces[i - 1][1])
@@ -180,9 +190,8 @@
             gate_values, up_values = scale * total[0], scale * total[1]
             s.g[me] = (gate_values / (1.0 + jnp.exp(-gate_values)) * up_values).astype(BF)
             gather_start(s)
-            if i > 0:
-                gather_forward(pieces[i - 1][1])
-        gather_forward(pieces[-1][1])
+        for _, s in pieces:
+            gather_forward(s)
         load_down.wait()
         acc = jnp.zeros((rows, width), F32)
         for (start, size), s in pieces:
@@ -192,10 +201,12 @@
 
     own_tp = pl.ds(pl.multiple_of(tp * rt, rt), rt)
     half_step(mem.first, arg.tokens[...], lambda: arg.tokens[own_tp], arg.gain_first, held.gate_first,
-              held.up_first, held.down_first, load.gate_first, load.up_first, load.down_first)
+              held.up_first, held.down_first, load.gate_first, load.up_first, load.down_first,
+              everyone_here)
 
     n = mem.mix
     norm_prepare(n, flat(mem.first.o), arg.gain_mix)
+    norm_send(n)
     dm = arg.w_query.shape[1]
     n_heads = arg.w_ingate.shape[0]
     one, two = n.parts
@@ -297,6 +308,28 @@
         copy.wait_send()
 
 
+def results_kernel(mixed, normalizer, stabilizer, memory, mixed_out, normalizer_out, stabilizer_out, memory_out,
+                   held, in_sem, out_sem):
+    count = in_sem.shape[0]
+    size = held.shape[0] // count
+
+    def piece(i):
+        return pl.ds(i * size, size)
+
+    ins = [pltpu.make_async_copy(memory.at[piece(i)], held.at[piece(i)], in_sem.at[i]) for i in range(count)]
+    outs = [pltpu.make_async_copy(held.at[piece(i)], memory_out.at[piece(i)], out_sem.at[i]) for i in range(count)]
+    for copy in ins:
+        copy.start()
+    mixed_out[...] = mixed[...]
+    normalizer_out[...] = normalizer[...]
+    stabilizer_out[...] = stabilizer[...]
+    for into, out in zip(ins, outs):
+        into.wait()
+        out.start()
+    for copy in outs:
+        copy.wait()
+
+
 def on_device(
     n_kv, n_tp, tokens, gain_first, gate_first, up_first, down_first, gain_mix, w_query, w_key, w_value,
     w_outgate, w_ingate, w_forget, forget_bias, memory, normalizer, stabilizer, w_project, gain_second,
@@ -396,6 +429,14 @@
         compiler_params=pltpu.CompilerParams(
             collective_id=0, has_side_effects=True, vmem_limit_bytes=60 * 2**20),
     )(*operands.values())
+    count = math.gcd(rb, 8)
+    mixed_out, normalizer_new, stabilizer_new, memory_new = pl.pallas_call(
+        results_kernel,
+        out_shape=[results[name] for name in ("mixed_out", "normalizer_new", "stabilizer_new", "memory_new")],
+        in_specs=[vm, vm, vm, hbm],
+        out_specs=[vm, vm, vm, hbm],
+        scratch_shapes=[pltpu.VMEM(memory.shape, F32), dma((count,)), dma((count,))],
+    )(mixed_out, normalizer_new, stabilizer_new, memory_new)
     return mixed_out, memory_new, normalizer_new, stabilizer_new.T
 
 

time: 118 us -> 115 us (0.975)
  local copies, waits for them, and re-layouts: 7.47 us -> 0 us
  Pallas kernels: 110 us -> 114 us
    unnamed x8 -> x0, local copies, waits for them, and re-layouts: 7.47 us -> none
    pallas_call x0 -> x1, Pallas kernels: none -> 5.17 us  [on_device(): pl.pallas_call(results_kernel, out_shape=[results[name] for name in ('mix...]
where the time goes in v1:
time: 115 us; the launch traced here: 114 us
  Pallas kernels  114 us (99%)
    pallas_call x1, Pallas kernels, on_device(): pl.pallas_call(functools.partial(layer_kernel, n_kv, n_tp, unpack), out_s...  109 us
    pallas_call x1, Pallas kernels, on_device(): pl.pallas_call(results_kernel, out_shape=[results[name] for name in ('mix...  5.17 us

profile of v1, /device:TPU:0, one launch (start us, length us, event | category | flops | bytes accessed | tf_op | source)
XLA Modules:
  0.0 114.4 jit_solution(9101476871941366283)
XLA Ops:
  0.6 108.6 %shard_map.228 = (bf16[128,512]{1,0:T(8,128)(2,1)}, f32[16,4,128,128]{3,2,1,0:T(8,128)}, f32[16,4,128]{2,1,0:T(4,128)}, f32[4,16]{1,0:T(4,128)}) custom-call(bf16[128,512]{1,0:T(8,128)(2,1)} %refs_0_.1, f32[1,512]{1,0:T(1,128)} %bitcast.17, f32[1,512]{1,0:T(1,128)} %bitcast.18, f32[1,512]{1,0:T(1,128)} %bitcast.19, bf16[16,512]{1,0:T(8,128)(2,1)} %bitcast.15, ...), custom_call_target="tpu_custom_call" | custom-call | tf_op jit(solution)/shard_map/pallas_call | solution.py:423
  109.3 5.2 %shard_map.229 = (bf16[128,512]{1,0:T(8,128)(2,1)}, f32[16,4,128]{2,1,0:T(4,128)}, f32[4,16]{1,0:T(4,128)}, f32[16,4,128,128]{3,2,1,0:T(8,128)}) custom-call(bf16[128,512]{1,0:T(8,128)(2,1)} %get-tuple-element.12.mixed, f32[16,4,128]{2,1,0:T(4,128)} %get-tuple-element.13.normalizer, f32[4,16]{1,0:T(4,128)} %get-tuple-element.14.stabilizer, ...), custom_call_target="tpu_custom_call" | custom-call | tf_op jit(solution)/shard_map/pallas_call | solution.py:433

commit v2 on v0

--- a/solution.py
+++ b/solution.py
@@ -1,4 +1,5 @@
 import functools
+import math
 from types import SimpleNamespace as NS
 
 import jax
@@ -47,7 +48,9 @@
         pl.semaphore_signal(barrier, inc=1, device_id={"kv": lax.rem(me + d, n_kv)}, device_id_type=MESH)
     for d in range(1, n_tp):
         pl.semaphore_signal(barrier, inc=1, device_id={"tp": lax.rem(tp + d, n_tp)}, device_id_type=MESH)
-    pl.semaphore_wait(barrier, n_kv + n_tp - 2)
+
+    def everyone_here():
+        pl.semaphore_wait(barrier, n_kv + n_tp - 2)
 
     pending = []
 
@@ -56,9 +59,8 @@
             src_ref=src, dst_ref=dst, send_sem=send_sem, recv_sem=recv_sem, device_id=where, device_id_type=MESH)
 
     def send(*args):
-        copy = remote(*args)
-        copy.start()
-        pending.append(copy)
+        remote(*args).start()
+        pending.append(args)
 
     def arrived(dst, send_sem, recv_sem):
         remote(dst, dst, send_sem, recv_sem, {"kv": partner}).wait_recv()
@@ -66,12 +68,17 @@
     def flat(ref):
         a, b, w = ref.shape
         return ref[...].reshape(a * b, w)
+
+    def rows_of(ref):
+        return lambda own=None: flat(ref) if own is None else ref[tp]
 
     def norm_prepare(n, x, gain):
         wide = x.astype(F32)
         mem.scaled[...] = (wide * gain[...]).astype(BF)
         part = jnp.sum(wide * wide, axis=1, keepdims=True)
         n.sq_out[...] = jnp.broadcast_to(part, (rows, LANES)).reshape(n_kv, rb, LANES)
+
+    def norm_send(n):
         for d in range(1, n_kv):
             peer = lax.rem(me + d, n_kv)
             send(n.sq_out.at[peer], n.sq_in.at[d], n.sq_s.at[d], n.sq_r.at[d], {"kv": peer})
@@ -142,7 +149,118 @@
             block = lax.rem(z - d - 1 + nz, nz) * 2 + 1 - c
             arrived(s.g.at[block], s.hs.at[d], s.hr.at[d])
 
+    line = nz == 4
+    at_end = (z == 0) | (z == nz - 1)
+    mate = z + 1 - 2 * lax.rem(z, 2)
+    far_middle = jnp.where(z < 2, 2, 1)
+    far_end = jnp.where(z < 2, 3, 0)
+    far = (far_middle, far_end)
+
+    def chip_sum(s, chip):
+        return s.a[c, chip].astype(F32) + s.b[chip].astype(F32)
+
+    def line_send_out(s):
+        for d in range(nz):
+            chip = lax.rem(z + d + 1, nz)
+            arrived(s.b.at[chip], s.s1.at[d], s.r1.at[d])
+
+        @pl.when(at_end)
+        def _():
+            for j in range(2):
+                s.c[j] = chip_sum(s, far[j]).astype(BF)
+                remote(s.c.at[j], s.e.at[j], s.s2.at[j], s.re.at[j], {"kv": mate * 2 + c}).start()
+
+        @pl.when(jnp.logical_not(at_end))
+        def _():
+            line_send_mate(s)
+
+    def line_send_mate(s):
+        s.c[2] = chip_sum(s, mate).astype(BF)
+        remote(s.c.at[2], s.d.at[0], s.s2.at[2], s.r2.at[0], {"kv": mate * 2 + c}).start()
+
+    def line_pass(s):
+        @pl.when(at_end)
+        def _():
+            line_send_mate(s)
+
+        @pl.when(jnp.logical_not(at_end))
+        def _():
+            for j in range(2):
+                arrived(s.e.at[j], s.s2.at[j], s.re.at[j])
+                s.c[j] = (chip_sum(s, far[j]) + s.e[j].astype(F32)).astype(BF)
+                remote(s.c.at[j], s.d.at[1], s.s2.at[j], s.r2.at[1], {"kv": far[j] * 2 + c}).start()
+
+        for j in range(3):
+            pending.append((s.c.at[j], s.d.at[0], s.s2.at[j], s.r2.at[0], {"kv": mate * 2 + c}))
+
+    def line_sum(s):
+        total = chip_sum(s, z)
+        for j in range(2):
+            arrived(s.d.at[j], s.s2.at[j], s.r2.at[j])
+            total = total + s.d[j].astype(F32)
+        return total
+
+    def line_gather_start(s):
+        send(s.g.at[me], s.g.at[me], s.gs.at[0], s.gr.at[0], {"kv": mate * 2 + c})
+        send(s.g.at[me], s.g.at[me], s.gs.at[1], s.gr.at[jnp.where(at_end, 2, 1)], {"kv": far_middle * 2 + c})
+        send(s.g.at[me], s.g.at[me], s.hs.at[nz - 1], s.hr.at[nz - 1], {"kv": partner})
+
+    def line_gather_forward(s):
+        for j, chip in enumerate((mate, far_middle, far_end)):
+            block = chip * 2 + c
+            arrived(s.g.at[block], s.gs.at[j], s.gr.at[j])
+            if j > 0:
+                @pl.when(jnp.logical_not(at_end))
+                def _():
+                    remote(s.g.at[block], s.g.at[block], s.gs.at[j + 1], s.gr.at[j], {"kv": mate * 2 + c}).start()
+            send(s.g.at[block], s.g.at[block], s.hs.at[j], s.hr.at[j], {"kv": partner})
+
+    def line_gather_wait(s):
+        for j, chip in enumerate((mate, far_middle, far_end, z)):
+            arrived(s.g.at[chip * 2 + 1 - c], s.hs.at[j], s.hr.at[j])
+
+    def line_gather_sent(s):
+        @pl.when(jnp.logical_not(at_end))
+        def _():
+            for j in range(1, 3):
+                block = far[j - 1] * 2 + c
+                remote(s.g.at[block], s.g.at[block], s.gs.at[j + 1], s.gr.at[j], {"kv": mate * 2 + c}).wait_send()
+
     def sum_tp(n, acc, residual, factor):
+        if n_tp == 4:
+            sum_tp_exchange(n, acc, residual(), factor)
+        else:
+            sum_tp_scatter(n, acc, residual(own_tp), factor)
+
+    def sum_tp_exchange(n, acc, residual, factor):
+        half = width // 2
+        sub = rows // 2
+        one, two = tp + 1 - 2 * lax.rem(tp, 2), lax.rem(tp + 2, 4)
+        order = [(k, r) for r in range(2) for k in range(2)]
+
+        def part(val, k, r):
+            return val[r * sub:(r + 1) * sub, k * half:(k + 1) * half]
+
+        def swap(step, k, r):
+            i = (step * 2 + k) * 2 + r
+            return n.p.at[i], n.q.at[i], n.ps.at[i], n.pr.at[i], {"tp": one if k == step else two}
+
+        for k, r in order:
+            n.p[k * 2 + r] = part(acc, k, r).astype(BF)
+            send(*swap(0, k, r))
+        for k, r in order:
+            i = k * 2 + r
+            arrived(n.q.at[i], n.ps.at[i], n.pr.at[i])
+            n.p[4 + i] = (n.p[i].astype(F32) + n.q[i].astype(F32)).astype(BF)
+            send(*swap(1, k, r))
+        for k, r in order:
+            i = 4 + k * 2 + r
+            arrived(n.q.at[i], n.ps.at[i], n.pr.at[i])
+            total = n.p[i].astype(F32) + n.q[i].astype(F32)
+            val = (part(residual, k, r).astype(F32) + factor * total).astype(BF)
+            n.o[r * 2:(r + 1) * 2, :, k * half:(k + 1) * half] = val.reshape(2, rt, half)
+
+    def sum_tp_scatter(n, acc, residual, factor):
         mem.acc[...] = acc
         for j in range(n_tp):
             n.p[j] = acc[j * rt:(j + 1) * rt].astype(BF)
@@ -161,8 +279,10 @@
             source = lax.rem(tp - d + n_tp, n_tp)
             arrived(n.o.at[source], n.os.at[d], n.ur.at[d])
 
-    def half_step(n, x, residual, gain, gate, up, down, load_gate, load_up, load_down):
+    def half_step(n, x, residual, gain, gate, up, down, load_gate, load_up, load_down, ready=None):
         norm_prepare(n, x, gain)
+        if ready is None:
+            norm_send(n)
         pieces = list(zip(chunks_of(gate.shape[0]), n.parts))
         load_gate.wait()
         for i, ((start, size), s) in enumerate(pieces):
@@ -170,32 +290,42 @@
             if i == 0:
                 load_up.wait()
             product(up, start, size, s.a, 1)
+            if i == 0 and ready is not None:
+                ready()
+                norm_send(n)
             scatter_pair(s)
             if i > 0:
-                scatter_chips(pieces[i - 1][1])
-        scatter_chips(pieces[-1][1])
+                (line_send_out if line else scatter_chips)(pieces[i - 1][1])
+        (line_send_out if line else scatter_chips)(pieces[-1][1])
         scale = norm_scale(n)
+        if line:
+            for _, s in pieces:
+                line_pass(s)
         for i, (_, s) in enumerate(pieces):
-            total = scatter_sum(s)
+            total = (line_sum if line else scatter_sum)(s)
             gate_values, up_values = scale * total[0], scale * total[1]
             s.g[me] = (gate_values / (1.0 + jnp.exp(-gate_values)) * up_values).astype(BF)
-            gather_start(s)
-            if i > 0:
-                gather_forward(pieces[i - 1][1])
-        gather_forward(pieces[-1][1])
+            (line_gather_start if line else gather_start)(s)
+        for _, s in pieces:
+            (line_gather_forward if line else gather_forward)(s)
         load_down.wait()
         acc = jnp.zeros((rows, width), F32)
         for (start, size), s in pieces:
-            gather_wait(s)
+            (line_gather_wait if line else gather_wait)(s)
             acc = acc + jnp.dot(flat(s.g), down[start:start + size, :], preferred_element_type=F32)
-        sum_tp(n, acc, residual(), 0.5)
+        sum_tp(n, acc, residual, 0.5)
+        if line:
+            for _, s in pieces:
+                line_gather_sent(s)
 
     own_tp = pl.ds(pl.multiple_of(tp * rt, rt), rt)
-    half_step(mem.first, arg.tokens[...], lambda: arg.tokens[own_tp], arg.gain_first, held.gate_first,
-              held.up_first, held.down_first, load.gate_first, load.up_first, load.down_first)
+    half_step(mem.first, arg.tokens[...], lambda own=slice(None): arg.tokens[own], arg.gain_first, held.gate_first,
+              held.up_first, held.down_first, load.gate_first, load.up_first, load.down_first,
+              everyone_here)
 
     n = mem.mix
     norm_prepare(n, flat(mem.first.o), arg.gain_mix)
+    norm_send(n)
     dm = arg.w_query.shape[1]
     n_heads = arg.w_ingate.shape[0]
     one, two = n.parts
@@ -287,14 +417,35 @@
     gather_forward(one)
     load.w_project.wait()
     gather_wait(one)
-    sum_tp(n, jnp.dot(flat(one.g), held.w_project[...], preferred_element_type=F32), mem.first.o[tp], 1.0)
-
-    half_step(mem.second, flat(n.o), lambda: n.o[tp], arg.gain_second, held.gate_second,
+    sum_tp(n, jnp.dot(flat(one.g), held.w_project[...], preferred_element_type=F32), rows_of(mem.first.o), 1.0)
+
+    half_step(mem.second, flat(n.o), rows_of(n.o), arg.gain_second, held.gate_second,
               held.up_second, held.down_second, load.gate_second, load.up_second, load.down_second)
     out.mixed_out[...] = flat(mem.second.o)
     store.wait()
-    for copy in pending:
-        copy.wait_send()
+    for args in pending:
+        remote(*args).wait_send()
+
+
+def results_kernel(count, n, *refs):
+    sources, targets, held, (in_sem, out_sem) = refs[:n], refs[n:2 * n], refs[2 * n:3 * n], refs[3 * n:]
+    pieces = []
+    for source, target, ref in zip(sources, targets, held):
+        cuts = count if source is sources[0] else 1
+        size = ref.shape[0] // cuts
+        for i in range(cuts):
+            at = pl.ds(i * size, size)
+            sems = len(pieces)
+            pieces.append((
+                pltpu.make_async_copy(source.at[at], ref.at[at], in_sem.at[sems]),
+                pltpu.make_async_copy(ref.at[at], target.at[at], out_sem.at[sems])))
+    for into, _ in pieces:
+        into.start()
+    for into, out in pieces:
+        into.wait()
+        out.start()
+    for _, out in pieces:
+        out.wait()
 
 
 def on_device(
@@ -330,19 +481,22 @@
             a=pltpu.VMEM((2, nz, g, rb, cols), BF), b=pltpu.VMEM((nz, g, rb, cols), BF),
             c=pltpu.VMEM((nz, g, rb, cols), BF), d=pltpu.VMEM((nz, g, rb, cols), BF),
             s1=dma((nz,)), r1=dma((nz,)), s2=dma((nz,)), r2=dma((nz,)))
+        if g == 2 and nz == 4:
+            bufs.update(e=pltpu.VMEM((2, g, rb, cols), BF), re=dma((2,)))
         if gathered:
             bufs.update(
                 g=pltpu.VMEM((n_kv, rb, gathered), BF), gs=dma((nz,)), gr=dma((nz,)), hs=dma((nz,)), hr=dma((nz,)))
         return bufs
+
+    swap = (8, rows // 2, width // 2) if n_tp == 4 else (n_tp, rt, width)
 
     def phase(parts):
         return dict(
             parts=parts,
             sq_out=pltpu.VMEM((n_kv, rb, LANES), F32), sq_in=pltpu.VMEM((n_kv, rb, LANES), F32),
             sq_s=dma((n_kv,)), sq_r=dma((n_kv,)),
-            p=pltpu.VMEM((n_tp, rt, width), BF), q=pltpu.VMEM((n_tp, rt, width), BF),
-            o=pltpu.VMEM((n_tp, rt, width), BF),
-            ps=dma((n_tp,)), pr=dma((n_tp,)), os=dma((n_tp,)), ur=dma((n_tp,)))
+            p=pltpu.VMEM(swap, BF), q=pltpu.VMEM(swap, BF), o=pltpu.VMEM((n_tp, rt, width), BF),
+            ps=dma(swap[:1]), pr=dma(swap[:1]), os=dma((n_tp,)), ur=dma((n_tp,)))
 
     tree = dict(
         held={name: pltpu.VMEM(a.shape, a.dtype) for name, a in streamed.items()},
@@ -396,6 +550,16 @@
         compiler_params=pltpu.CompilerParams(
             collective_id=0, has_side_effects=True, vmem_limit_bytes=60 * 2**20),
     )(*operands.values())
+    count = math.gcd(rb, 8)
+    passed = [memory_new, mixed_out, normalizer_new, stabilizer_new]
+    memory_new, mixed_out, normalizer_new, stabilizer_new = pl.pallas_call(
+        functools.partial(results_kernel, count, len(passed)),
+        out_shape=[jax.ShapeDtypeStruct(a.shape, a.dtype) for a in passed],
+        in_specs=[hbm] * len(passed),
+        out_specs=[hbm] * len(passed),
+        scratch_shapes=[pltpu.VMEM(a.shape, a.dtype) for a in passed]
+        + [dma((count + len(passed) - 1,)), dma((count + len(passed) - 1,))],
+    )(*passed)
     return mixed_out, memory_new, normalizer_new, stabilizer_new.T
 
 

time: 118 us -> 101 us (0.86)
  Pallas kernels: 110 us -> 100 us
  local copies, waits for them, and re-layouts: 7.47 us -> 0 us
    pallas_call x1, Pallas kernels: 110 us -> 96.3 us  [on_device(): pl.pallas_call(functools.partial(layer_kernel, n_kv, n_tp, unpack), out_s...]
    unnamed x8 -> x0, local copies, waits for them, and re-layouts: 7.47 us -> none
    pallas_call x0 -> x1, Pallas kernels: none -> 3.67 us  [on_device(): pl.pallas_call(functools.partial(results_kernel, count, len(passed)), out...]
where the time goes in v2:
time: 101 us
  Pallas kernels  100 us (99%)
    pallas_call x1, Pallas kernels, on_device(): pl.pallas_call(functools.partial(layer_kernel, n_kv, n_tp, unpack), out_s...  96.3 us
    pallas_call x1, Pallas kernels, on_device(): pl.pallas_call(functools.partial(results_kernel, count, len(passed)), out...  3.67 us

profile of v2, /device:TPU:0, one launch (start us, length us, event | category | flops | bytes accessed | tf_op | source)
XLA Modules:
  0.0 100.6 jit_solution(10022936793614534641)
XLA Ops:
  0.6 96.3 %shard_map.228 = (bf16[128,512]{1,0:T(8,128)(2,1)}, f32[16,4,128,128]{3,2,1,0:T(8,128)}, f32[16,4,128]{2,1,0:T(4,128)}, f32[4,16]{1,0:T(4,128)}) custom-call(bf16[128,512]{1,0:T(8,128)(2,1)} %refs_0_.1, f32[1,512]{1,0:T(1,128)} %bitcast.17, f32[1,512]{1,0:T(1,128)} %bitcast.18, f32[1,512]{1,0:T(1,128)} %bitcast.19, bf16[16,512]{1,0:T(8,128)(2,1)} %bitcast.15, ...), custom_call_target="tpu_custom_call" | custom-call | tf_op jit(solution)/shard_map/pallas_call | solution.py:544
  97.0 3.7 %shard_map.229 = (f32[16,4,128,128]{3,2,1,0:T(8,128)}, bf16[128,512]{1,0:T(8,128)(2,1)}, f32[16,4,128]{2,1,0:T(4,128)}, f32[4,16]{1,0:T(4,128)}) custom-call(f32[16,4,128,128]{3,2,1,0:T(8,128)} %get-tuple-element.12.refs_0_, bf16[128,512]{1,0:T(8,128)(2,1)} %get-tuple-element.13.refs_1_, f32[16,4,128]{2,1,0:T(4,128)} %get-tuple-element.14.refs_2_, ...), custom_call_target="tpu_custom_call" | custom-call | tf_op jit(solution)/shard_map/pallas_call | solution.py:555

commit v3 on v2

--- a/solution.py
+++ b/solution.py
@@ -11,15 +11,26 @@
 
 EPSILON = 1e-06
 LANES = 128
-CHUNKS = 4
+TILE = 256
+PACE = (3, 3, 3, 2)
+DIRECT = 1
+LAG = 9
+READY = 0
+BLOCKS = 4
 MESH = pl.DeviceIdType.MESH
 BF = jnp.bfloat16
 F32 = jnp.float32
 
 
 def chunks_of(hidden):
-    size = -(-hidden // (CHUNKS * 256)) * 256
-    return [(at, min(size, hidden - at)) for at in range(0, hidden, size)]
+    tiles = -(-hidden // TILE)
+    total, passed, cuts = sum(PACE), 0, [0]
+    for share in PACE:
+        passed += share
+        cut = min(hidden, (tiles * passed + total // 2) // total * TILE)
+        if cut > cuts[-1]:
+            cuts.append(cut)
+    return [(low, high - low) for low, high in zip(cuts, cuts[1:])]
 
 
 def layer_kernel(n_kv, n_tp, unpack, *refs):
@@ -36,12 +47,32 @@
     head_size = arg.memory.shape[-1]
     heads = arg.memory.shape[1]
 
+    pieces_of = chunks_of(arg.gate_first.shape[0])
+    relayed = max(len(pieces_of) - DIRECT, 0)
+    held = NS(**mem.held)
     loads = {}
-    for i, (name, ref) in enumerate(mem.held.items()):
-        loads[name] = pltpu.make_async_copy(getattr(arg, name), ref, mem.load_sem.at[i])
-        loads[name].start()
-    held = NS(**mem.held)
-    load = NS(**loads)
+
+    def begin(name, cuts=None):
+        source, target = getattr(arg, name), mem.held[name]
+        for cut in cuts or [None]:
+            at = slice(None) if cut is None else pl.ds(*cut)
+            sem = mem.load_sem.at[sum(len(made) for made in loads.values())]
+            copy = pltpu.make_async_copy(source.at[at], target.at[at], sem)
+            copy.start()
+            loads.setdefault(name, []).append(copy)
+
+    def loaded(name, i=None):
+        for copy in loads[name] if i is None else [loads[name][i]]:
+            copy.wait()
+
+    begin("tokens")
+    begin("gain_first")
+    for cut in pieces_of:
+        begin("gate_first", [cut])
+        begin("up_first", [cut])
+    for name in mem.held:
+        if name not in loads:
+            begin(name)
 
     barrier = pltpu.get_barrier_semaphore()
     for d in range(1, n_kv):
@@ -99,7 +130,7 @@
             buf[i % 2, i // 2, g, :, place] = val[i * rb:(i + 1) * rb]
 
     def product(weight, start, size, buf, g):
-        step = 256
+        step = TILE
         full = size // step
 
         def tile(off, n, place):
@@ -166,7 +197,7 @@
 
         @pl.when(at_end)
         def _():
-            for j in range(2):
+            for j in (1, 0):
                 s.c[j] = chip_sum(s, far[j]).astype(BF)
                 remote(s.c.at[j], s.e.at[j], s.s2.at[j], s.re.at[j], {"kv": mate * 2 + c}).start()
 
@@ -178,14 +209,15 @@
         s.c[2] = chip_sum(s, mate).astype(BF)
         remote(s.c.at[2], s.d.at[0], s.s2.at[2], s.r2.at[0], {"kv": mate * 2 + c}).start()
 
-    def line_pass(s):
+    def line_follow(s):
         @pl.when(at_end)
         def _():
             line_send_mate(s)
 
+    def line_pass(s):
         @pl.when(jnp.logical_not(at_end))
         def _():
-            for j in range(2):
+            for j in (1, 0):
                 arrived(s.e.at[j], s.s2.at[j], s.re.at[j])
                 s.c[j] = (chip_sum(s, far[j]) + s.e[j].astype(F32)).astype(BF)
                 remote(s.c.at[j], s.d.at[1], s.s2.at[j], s.r2.at[1], {"kv": far[j] * 2 + c}).start()
@@ -200,16 +232,19 @@
             total = total + s.d[j].astype(F32)
         return total
 
-    def line_gather_start(s):
+    mine = jnp.where(at_end, 2, 1)
+
+    def line_gather_start(s, direct):
         send(s.g.at[me], s.g.at[me], s.gs.at[0], s.gr.at[0], {"kv": mate * 2 + c})
-        send(s.g.at[me], s.g.at[me], s.gs.at[1], s.gr.at[jnp.where(at_end, 2, 1)], {"kv": far_middle * 2 + c})
+        for j in range(2 if direct else 1):
+            send(s.g.at[me], s.g.at[me], s.gs.at[1 + j], s.gr.at[mine], {"kv": far[j] * 2 + c})
         send(s.g.at[me], s.g.at[me], s.hs.at[nz - 1], s.hr.at[nz - 1], {"kv": partner})
 
-    def line_gather_forward(s):
+    def line_gather_forward(s, direct):
         for j, chip in enumerate((mate, far_middle, far_end)):
             block = chip * 2 + c
             arrived(s.g.at[block], s.gs.at[j], s.gr.at[j])
-            if j > 0:
+            if j > 0 and not direct:
                 @pl.when(jnp.logical_not(at_end))
                 def _():
                     remote(s.g.at[block], s.g.at[block], s.gs.at[j + 1], s.gr.at[j], {"kv": mate * 2 + c}).start()
@@ -227,38 +262,38 @@
                 remote(s.g.at[block], s.g.at[block], s.gs.at[j + 1], s.gr.at[j], {"kv": mate * 2 + c}).wait_send()
 
     def sum_tp(n, acc, residual, factor):
-        if n_tp == 4:
+        if n_tp == BLOCKS:
             sum_tp_exchange(n, acc, residual(), factor)
         else:
             sum_tp_scatter(n, acc, residual(own_tp), factor)
 
     def sum_tp_exchange(n, acc, residual, factor):
         half = width // 2
-        sub = rows // 2
+        sub = rows // BLOCKS
         one, two = tp + 1 - 2 * lax.rem(tp, 2), lax.rem(tp + 2, 4)
-        order = [(k, r) for r in range(2) for k in range(2)]
+        order = [(k, r) for r in range(BLOCKS) for k in range(2)]
 
         def part(val, k, r):
             return val[r * sub:(r + 1) * sub, k * half:(k + 1) * half]
 
         def swap(step, k, r):
-            i = (step * 2 + k) * 2 + r
+            i = (step * 2 + k) * BLOCKS + r
             return n.p.at[i], n.q.at[i], n.ps.at[i], n.pr.at[i], {"tp": one if k == step else two}
 
         for k, r in order:
-            n.p[k * 2 + r] = part(acc, k, r).astype(BF)
+            n.p[k * BLOCKS + r] = part(acc, k, r).astype(BF)
             send(*swap(0, k, r))
         for k, r in order:
-            i = k * 2 + r
+            i = k * BLOCKS + r
             arrived(n.q.at[i], n.ps.at[i], n.pr.at[i])
-            n.p[4 + i] = (n.p[i].astype(F32) + n.q[i].astype(F32)).astype(BF)
+            n.p[2 * BLOCKS + i] = (n.p[i].astype(F32) + n.q[i].astype(F32)).astype(BF)
             send(*swap(1, k, r))
         for k, r in order:
-            i = 4 + k * 2 + r
+            i = (2 + k) * BLOCKS + r
             arrived(n.q.at[i], n.ps.at[i], n.pr.at[i])
             total = n.p[i].astype(F32) + n.q[i].astype(F32)
             val = (part(residual, k, r).astype(F32) + factor * total).astype(BF)
-            n.o[r * 2:(r + 1) * 2, :, k * half:(k + 1) * half] = val.reshape(2, rt, half)
+            n.o[r, :, k * half:(k + 1) * half] = val
 
     def sum_tp_scatter(n, acc, residual, factor):
         mem.acc[...] = acc
@@ -279,72 +314,98 @@
             source = lax.rem(tp - d + n_tp, n_tp)
             arrived(n.o.at[source], n.os.at[d], n.ur.at[d])
 
-    def half_step(n, x, residual, gain, gate, up, down, load_gate, load_up, load_down, ready=None):
-        norm_prepare(n, x, gain)
+    def send_out(pieces, i):
+        if not line:
+            scatter_chips(pieces[i][1])
+            return
+        line_send_out(pieces[i][1])
+        if i >= LAG:
+            line_follow(pieces[i - LAG][1])
+
+    def half_step(label, n, x, residual, ready=None):
+        gate, up, down = (mem.held[name + label] for name in ("gate_", "up_", "down_"))
+        norm_prepare(n, x, mem.held["gain_" + label])
         if ready is None:
             norm_send(n)
-        pieces = list(zip(chunks_of(gate.shape[0]), n.parts))
-        load_gate.wait()
+        pieces = list(zip(pieces_of, n.parts))
+        by_piece = len(loads["gate_" + label]) > 1
+        held_back = min(READY, len(pieces) - 1)
         for i, ((start, size), s) in enumerate(pieces):
+            if by_piece or i == 0:
+                loaded("gate_" + label, i)
             product(gate, start, size, s.a, 0)
-            if i == 0:
-                load_up.wait()
+            if by_piece or i == 0:
+                loaded("up_" + label, i)
             product(up, start, size, s.a, 1)
-            if i == 0 and ready is not None:
+            if ready is not None and i < held_back:
+                continue
+            if ready is not None and i == held_back:
                 ready()
                 norm_send(n)
+                for _, earlier in pieces[:i]:
+                    scatter_pair(earlier)
             scatter_pair(s)
-            if i > 0:
-                (line_send_out if line else scatter_chips)(pieces[i - 1][1])
-        (line_send_out if line else scatter_chips)(pieces[-1][1])
+            for j in range(0 if i == held_back and ready is not None else max(i - 1, 0), i):
+                send_out(pieces, j)
+        send_out(pieces, len(pieces) - 1)
         scale = norm_scale(n)
         if line:
+            for _, s in pieces[max(len(pieces) - LAG, 0):]:
+                line_follow(s)
             for _, s in pieces:
                 line_pass(s)
         for i, (_, s) in enumerate(pieces):
             total = (line_sum if line else scatter_sum)(s)
             gate_values, up_values = scale * total[0], scale * total[1]
             s.g[me] = (gate_values / (1.0 + jnp.exp(-gate_values)) * up_values).astype(BF)
-            (line_gather_start if line else gather_start)(s)
-        for _, s in pieces:
-            (line_gather_forward if line else gather_forward)(s)
-        load_down.wait()
+            if line:
+                line_gather_start(s, i >= relayed)
+            else:
+                gather_start(s)
+        for i, (_, s) in enumerate(pieces):
+            if line:
+                line_gather_forward(s, i >= relayed)
+            else:
+                gather_forward(s)
+        loaded("down_" + label)
         acc = jnp.zeros((rows, width), F32)
         for (start, size), s in pieces:
             (line_gather_wait if line else gather_wait)(s)
             acc = acc + jnp.dot(flat(s.g), down[start:start + size, :], preferred_element_type=F32)
         sum_tp(n, acc, residual, 0.5)
         if line:
-            for _, s in pieces:
+            for _, s in pieces[:relayed]:
                 line_gather_sent(s)
 
     own_tp = pl.ds(pl.multiple_of(tp * rt, rt), rt)
-    half_step(mem.first, arg.tokens[...], lambda own=slice(None): arg.tokens[own], arg.gain_first, held.gate_first,
-              held.up_first, held.down_first, load.gate_first, load.up_first, load.down_first,
-              everyone_here)
+    loaded("tokens")
+    loaded("gain_first")
+    half_step("first", mem.first, held.tokens[...], lambda own=slice(None): held.tokens[own], everyone_here)
+    for name in ("gain_mix", "w_ingate", "w_forget", "normalizer", "stabilizer", "gain_second"):
+        loaded(name)
 
     n = mem.mix
-    norm_prepare(n, flat(mem.first.o), arg.gain_mix)
+    norm_prepare(n, flat(mem.first.o), held.gain_mix)
     norm_send(n)
-    dm = arg.w_query.shape[1]
-    n_heads = arg.w_ingate.shape[0]
+    dm = held.w_query.shape[1]
+    n_heads = held.w_ingate.shape[0]
     one, two = n.parts
 
     def wide_product(weight, s, at):
         val = jnp.dot(mem.scaled[...], weight[...], preferred_element_type=F32).astype(BF)
         keep(s.a, 0, val, slice(at, at + dm))
 
-    load.w_query.wait()
+    loaded("w_query")
     wide_product(held.w_query, one, 0)
-    load.w_key.wait()
+    loaded("w_key")
     wide_product(held.w_key, one, dm)
-    gates = rows_dot(jnp.concatenate([arg.w_ingate[...], arg.w_forget[...]], axis=0))
+    gates = rows_dot(jnp.concatenate([held.w_ingate[...], held.w_forget[...]], axis=0))
     gates = jnp.concatenate([gates, jnp.zeros((rows, LANES - 2 * n_heads), BF)], axis=1)
     keep(one.a, 0, gates, slice(2 * dm, 2 * dm + LANES))
     scatter_pair(one)
-    load.w_value.wait()
+    loaded("w_value")
     wide_product(held.w_value, two, 0)
-    load.w_outgate.wait()
+    loaded("w_outgate")
     wide_product(held.w_outgate, two, dm)
     scatter_pair(two)
     scatter_chips(one)
@@ -356,7 +417,7 @@
     gates = total[:, 2 * dm:]
     lane = lax.broadcasted_iota(jnp.int32, (rb, LANES), 1)
     diagonal = lax.broadcasted_iota(jnp.int32, (rb, rb), 0) == lax.broadcasted_iota(jnp.int32, (rb, rb), 1)
-    load.memory.wait()
+    loaded("memory")
     state = held.memory
     parts = []
     for h in range(heads):
@@ -370,13 +431,13 @@
         forget = jnp.sum(jnp.where(lane == n_heads + tp * heads + h, gates, 0.0), axis=1, keepdims=True)
         forget = forget + arg.forget_bias[h]
         log_forget = jnp.minimum(forget, 0.0) - jnp.log1p(jnp.exp(-jnp.abs(forget)))
-        stabilizer = jnp.sum(jnp.where(diagonal, arg.stabilizer[h:h + 1, :], 0.0), axis=1, keepdims=True)
+        stabilizer = jnp.sum(jnp.where(diagonal, held.stabilizer[h:h + 1, :], 0.0), axis=1, keepdims=True)
         kept = log_forget + stabilizer
         ceiling = jnp.maximum(kept, ingate)
         fresh = jnp.exp(ingate - ceiling)
         carried = jnp.exp(kept - ceiling)
         out.stabilizer_new[h:h + 1, :] = jnp.sum(jnp.where(diagonal, ceiling, 0.0), axis=0, keepdims=True)
-        norm = arg.normalizer[:, h, :]
+        norm = held.normalizer[:, h, :]
         out.normalizer_new[:, h, :] = carried * norm + fresh * k
         own = jnp.sum(q * k, axis=1, keepdims=True) * fresh
         den = own + carried * jnp.sum(norm * q, axis=1, keepdims=True)
@@ -386,20 +447,28 @@
         mem.row_c[h] = jnp.broadcast_to(carried, (rb, head_size))
         pad = jnp.zeros((LANES - rb, head_size), F32)
         mem.col_v[h] = jnp.concatenate([v, pad], axis=0).T
-        mem.col_r[h] = jnp.zeros((head_size, LANES), F32)
         parts.append((own, v, carried, den, gate_out))
 
     lane2 = lax.broadcasted_iota(jnp.int32, (head_size, LANES), 1)
-
-    @pl.loop(0, rb)
-    def _(b):
-        for h in range(heads):
-            recall = jnp.sum(state[b, h] * mem.row_q[h, pl.ds(b, 1), :], axis=1, keepdims=True)
-            mem.col_r[h] = jnp.where(lane2 == b, recall, mem.col_r[h])
+    row = lax.broadcasted_iota(jnp.int32, (rb, head_size), 0)
+    queries = [mem.row_q[h].astype(BF) for h in range(heads)]
+    together = math.gcd(rb, 4)
+
+    def recall_step(step, found):
+        for at in range(together):
+            b = step * together + at
+            found = tuple(
+                jnp.where(row == b, lax.dot_general(
+                    queries[h], state[b, h].astype(BF), (((1,), (1,)), ((), ())), preferred_element_type=F32), found[h])
+                for h in range(heads))
+        return found
+
+    nothing = jnp.zeros((rb, head_size), F32)
+    recalls = lax.fori_loop(0, rb // together, recall_step, (nothing,) * heads)
 
     for h in range(heads):
         own, v, carried, den, gate_out = parts[h]
-        recall = mem.col_r[h].T[:rb]
+        recall = recalls[h]
         readout = (own * v + carried * recall) / den
         n.parts[0].g[me, :, h * head_size:(h + 1) * head_size] = (
             readout / (1.0 + jnp.exp(-gate_out))).astype(BF)
@@ -412,15 +481,14 @@
             state[b, h] = (mem.row_c[h, pl.ds(b, 1), :] * state[b, h]
                            + v_col * mem.row_k[h, pl.ds(b, 1), :])
 
-    store = pltpu.make_async_copy(state, out.memory_new, mem.load_sem.at[len(mem.held)])
+    store = pltpu.make_async_copy(state, out.memory_new, mem.load_sem.at[sum(len(made) for made in loads.values())])
     store.start()
     gather_forward(one)
-    load.w_project.wait()
+    loaded("w_project")
     gather_wait(one)
     sum_tp(n, jnp.dot(flat(one.g), held.w_project[...], preferred_element_type=F32), rows_of(mem.first.o), 1.0)
 
-    half_step(mem.second, flat(n.o), rows_of(n.o), arg.gain_second, held.gate_second,
-              held.up_second, held.down_second, load.gate_second, load.up_second, load.down_second)
+    half_step("second", mem.second, flat(n.o), rows_of(n.o))
     out.mixed_out[...] = flat(mem.second.o)
     store.wait()
     for args in pending:
@@ -460,16 +528,14 @@
     heads, head_size = memory.shape[1], memory.shape[3]
     dma = pltpu.SemaphoreType.DMA
 
-    in_vmem = dict(
-        tokens=tokens, gain_first=gain_first.reshape(1, -1), gain_mix=gain_mix.reshape(1, -1),
-        gain_second=gain_second.reshape(1, -1), w_ingate=w_ingate.T, w_forget=w_forget.T,
-        normalizer=normalizer, stabilizer=stabilizer.T)
     in_smem = dict(forget_bias=forget_bias)
     streamed = dict(
-        gate_first=gate_first.T, up_first=up_first.T, down_first=down_first, w_query=w_query, w_key=w_key,
-        w_value=w_value, w_outgate=w_outgate, memory=memory, w_project=w_project, gate_second=gate_second.T,
-        up_second=up_second.T, down_second=down_second)
-    operands = {**in_vmem, **in_smem, **streamed}
+        tokens=tokens, gain_first=gain_first.reshape(1, -1), gate_first=gate_first.T, up_first=up_first.T,
+        down_first=down_first, gain_mix=gain_mix.reshape(1, -1), w_ingate=w_ingate.T, w_forget=w_forget.T,
+        w_query=w_query, w_key=w_key, w_value=w_value, w_outgate=w_outgate, normalizer=normalizer,
+        stabilizer=stabilizer.T, memory=memory, w_project=w_project, gain_second=gain_second.reshape(1, -1),
+        gate_second=gate_second.T, up_second=up_second.T, down_second=down_second)
+    operands = {**in_smem, **streamed}
     results = dict(
         mixed_out=jax.ShapeDtypeStruct(tokens.shape, BF),
         memory_new=jax.ShapeDtypeStruct(memory.shape, F32),
@@ -488,7 +554,7 @@
                 g=pltpu.VMEM((n_kv, rb, gathered), BF), gs=dma((nz,)), gr=dma((nz,)), hs=dma((nz,)), hr=dma((nz,)))
         return bufs
 
-    swap = (8, rows // 2, width // 2) if n_tp == 4 else (n_tp, rt, width)
+    swap = (4 * BLOCKS, rows // BLOCKS, width // 2) if n_tp == BLOCKS else (n_tp, rt, width)
 
     def phase(parts):
         return dict(
@@ -500,7 +566,7 @@
 
     tree = dict(
         held={name: pltpu.VMEM(a.shape, a.dtype) for name, a in streamed.items()},
-        load_sem=dma((len(streamed) + 1,)),
+        load_sem=dma((len(streamed) + 2 * len(chunks_of(hidden)),)),
         scaled=pltpu.VMEM((rows, width), BF),
         acc=pltpu.VMEM((rows, width), F32),
         first=phase([exchange(2, size, size) for _, size in chunks_of(hidden)]),
@@ -509,8 +575,7 @@
         row_q=pltpu.VMEM((heads, rb, head_size), F32),
         row_k=pltpu.VMEM((heads, rb, head_size), F32),
         row_c=pltpu.VMEM((heads, rb, head_size), F32),
-        col_v=pltpu.VMEM((heads, head_size, LANES), F32),
-        col_r=pltpu.VMEM((heads, head_size, LANES), F32))
+        col_v=pltpu.VMEM((heads, head_size, LANES), F32))
 
     shapes = []
 
@@ -544,7 +609,7 @@
     mixed_out, memory_new, normalizer_new, stabilizer_new = pl.pallas_call(
         functools.partial(layer_kernel, n_kv, n_tp, unpack),
         out_shape=list(results.values()),
-        in_specs=[vm] * len(in_vmem) + [pl.BlockSpec(memory_space=pltpu.SMEM)] + [hbm] * len(streamed),
+        in_specs=[pl.BlockSpec(memory_space=pltpu.SMEM)] + [hbm] * len(streamed),
         out_specs=[vm, hbm, vm, vm],
         scratch_shapes=shapes,
         compiler_params=pltpu.CompilerParams(

time: 101 us -> 98.2 us (0.972)
  Pallas kernels: 100 us -> 97.4 us
    pallas_call x1, Pallas kernels: 96.3 us -> 93.7 us  [on_device(): pl.pallas_call(functools.partial(layer_kernel, n_kv, n_tp, unpack), out_s...]
where the time goes in v3:
time: 98.2 us; the launch traced here: 98 us
  Pallas kernels  97.4 us (99%)
    pallas_call x1, Pallas kernels, on_device(): pl.pallas_call(functools.partial(layer_kernel, n_kv, n_tp, unpack), out_s...  93.7 us
    pallas_call x1, Pallas kernels, on_device(): pl.pallas_call(functools.partial(results_kernel, count, len(passed)), out...  3.67 us

profile of v3, /device:TPU:0, one launch (start us, length us, event | category | flops | bytes accessed | tf_op | source)
XLA Modules:
  0.0 98.0 jit_solution(13418258407312602925)
XLA Ops:
  0.6 93.7 %shard_map.228 = (bf16[128,512]{1,0:T(8,128)(2,1)}, f32[16,4,128,128]{3,2,1,0:T(8,128)}, f32[16,4,128]{2,1,0:T(4,128)}, f32[4,16]{1,0:T(4,128)}) custom-call(f32[4]{0:T(128)} %refs_0_.1, bf16[128,512]{1,0:T(8,128)(2,1)} %refs_1_.1, f32[1,512]{1,0:T(1,128)} %bitcast.17, bf16[2752,512]{1,0:T(8,128)(2,1)} %bitcast.11, bf16[2752,512]{1,0:T(8,128)(2,1)} %bitcast.12, ...), custom_call_target="tpu_custom_call" | custom-call | tf_op jit(solution)/shard_map/pallas_call | solution.py:609
  94.3 3.7 %shard_map.229 = (f32[16,4,128,128]{3,2,1,0:T(8,128)}, bf16[128,512]{1,0:T(8,128)(2,1)}, f32[16,4,128]{2,1,0:T(4,128)}, f32[4,16]{1,0:T(4,128)}) custom-call(f32[16,4,128,128]{3,2,1,0:T(8,128)} %get-tuple-element.12.refs_0_, bf16[128,512]{1,0:T(8,128)(2,1)} %get-tuple-element.13.refs_1_, f32[16,4,128]{2,1,0:T(4,128)} %get-tuple-element.14.refs_2_, ...), custom_call_target="tpu_custom_call" | custom-call | tf_op jit(solution)/shard_map/pallas_call | solution.py:620

commit v4 on v3

--- a/solution.py
+++ b/solution.py
@@ -12,9 +12,10 @@
 EPSILON = 1e-06
 LANES = 128
 TILE = 256
-PACE = (3, 3, 3, 2)
+PACE = (2, 3, 3, 3)
 DIRECT = 1
 LAG = 9
+JOINED = 0
 READY = 0
 BLOCKS = 4
 MESH = pl.DeviceIdType.MESH
@@ -93,6 +94,11 @@
         remote(*args).start()
         pending.append(args)
 
+    def drain():
+        for args in pending:
+            remote(*args).wait_send()
+        pending.clear()
+
     def arrived(dst, send_sem, recv_sem):
         remote(dst, dst, send_sem, recv_sem, {"kv": partner}).wait_recv()
 
@@ -190,16 +196,23 @@
     def chip_sum(s, chip):
         return s.a[c, chip].astype(F32) + s.b[chip].astype(F32)
 
+    def line_pair(s):
+        send(s.a.at[1 - c], s.b, s.s1.at[0], s.r1.at[0], {"kv": partner})
+
     def line_send_out(s):
-        for d in range(nz):
-            chip = lax.rem(z + d + 1, nz)
-            arrived(s.b.at[chip], s.s1.at[d], s.r1.at[d])
+        arrived(s.b, s.s1.at[0], s.r1.at[0])
 
         @pl.when(at_end)
         def _():
-            for j in (1, 0):
-                s.c[j] = chip_sum(s, far[j]).astype(BF)
-                remote(s.c.at[j], s.e.at[j], s.s2.at[j], s.re.at[j], {"kv": mate * 2 + c}).start()
+            if JOINED:
+                for j in (1, 0):
+                    s.c[j] = chip_sum(s, far[j]).astype(BF)
+                both = pl.ds(0, 2)
+                remote(s.c.at[both], s.e, s.s2.at[0], s.re.at[0], {"kv": mate * 2 + c}).start()
+            else:
+                for j in (1, 0):
+                    s.c[j] = chip_sum(s, far[j]).astype(BF)
+                    remote(s.c.at[j], s.e.at[j], s.s2.at[j], s.re.at[j], {"kv": mate * 2 + c}).start()
 
         @pl.when(jnp.logical_not(at_end))
         def _():
@@ -265,6 +278,7 @@
         if n_tp == BLOCKS:
             sum_tp_exchange(n, acc, residual(), factor)
         else:
+            drain()
             sum_tp_scatter(n, acc, residual(own_tp), factor)
 
     def sum_tp_exchange(n, acc, residual, factor):
@@ -283,6 +297,10 @@
         for k, r in order:
             n.p[k * BLOCKS + r] = part(acc, k, r).astype(BF)
             send(*swap(0, k, r))
+        started = pending[-len(order):]
+        del pending[-len(order):]
+        drain()
+        pending.extend(started)
         for k, r in order:
             i = k * BLOCKS + r
             arrived(n.q.at[i], n.ps.at[i], n.pr.at[i])
@@ -329,6 +347,7 @@
             norm_send(n)
         pieces = list(zip(pieces_of, n.parts))
         by_piece = len(loads["gate_" + label]) > 1
+        pair = line_pair if line else scatter_pair
         held_back = min(READY, len(pieces) - 1)
         for i, ((start, size), s) in enumerate(pieces):
             if by_piece or i == 0:
@@ -343,12 +362,13 @@
                 ready()
                 norm_send(n)
                 for _, earlier in pieces[:i]:
-                    scatter_pair(earlier)
-            scatter_pair(s)
+                    pair(earlier)
+            pair(s)
             for j in range(0 if i == held_back and ready is not None else max(i - 1, 0), i):
                 send_out(pieces, j)
         send_out(pieces, len(pieces) - 1)
         scale = norm_scale(n)
+        drain()
         if line:
             for _, s in pieces[max(len(pieces) - LAG, 0):]:
                 line_follow(s)
@@ -491,8 +511,7 @@
     half_step("second", mem.second, flat(n.o), rows_of(n.o))
     out.mixed_out[...] = flat(mem.second.o)
     store.wait()
-    for args in pending:
-        remote(*args).wait_send()
+    drain()
 
 
 def results_kernel(count, n, *refs):
@@ -542,36 +561,56 @@
         normalizer_new=jax.ShapeDtypeStruct(normalizer.shape, F32),
         stabilizer_new=jax.ShapeDtypeStruct(stabilizer.shape[::-1], F32))
 
-    def exchange(g, cols, gathered):
+    line = nz == 4
+
+    def signals(joined, gathered):
+        counts = dict(s1=nz, r1=nz, s2=nz, r2=nz)
+        if gathered:
+            counts.update(gs=nz, gr=nz, hs=nz, hr=nz)
+        if joined and line:
+            counts.update(s1=1, r1=1, s2=3, r2=2, re=2, gr=3)
+        return {name: dma((count,)) for name, count in counts.items()}
+
+    def exchange(g, cols, gathered, sems):
         bufs = dict(
             a=pltpu.VMEM((2, nz, g, rb, cols), BF), b=pltpu.VMEM((nz, g, rb, cols), BF),
-            c=pltpu.VMEM((nz, g, rb, cols), BF), d=pltpu.VMEM((nz, g, rb, cols), BF),
-            s1=dma((nz,)), r1=dma((nz,)), s2=dma((nz,)), r2=dma((nz,)))
-        if g == 2 and nz == 4:
-            bufs.update(e=pltpu.VMEM((2, g, rb, cols), BF), re=dma((2,)))
+            c=pltpu.VMEM((nz, g, rb, cols), BF), d=pltpu.VMEM((nz, g, rb, cols), BF), **sems)
+        if g == 2 and line:
+            bufs.update(e=pltpu.VMEM((2, g, rb, cols), BF))
         if gathered:
-            bufs.update(
-                g=pltpu.VMEM((n_kv, rb, gathered), BF), gs=dma((nz,)), gr=dma((nz,)), hs=dma((nz,)), hr=dma((nz,)))
+            bufs.update(g=pltpu.VMEM((n_kv, rb, gathered), BF))
         return bufs
 
-    swap = (4 * BLOCKS, rows // BLOCKS, width // 2) if n_tp == BLOCKS else (n_tp, rt, width)
-
-    def phase(parts):
+    traded = n_tp == BLOCKS
+    swap = (4 * BLOCKS, rows // BLOCKS, width // 2) if traded else (n_tp, rt, width)
+    squares = dict(sq_s=dma((n_kv,)), sq_r=dma((n_kv,)))
+
+    def sums():
+        made = dict(ps=dma(swap[:1]), pr=dma(swap[:1]))
+        return made if traded else dict(os=dma((n_tp,)), ur=dma((n_tp,)), **made)
+
+    def phase(parts, tp_sems):
         return dict(
             parts=parts,
             sq_out=pltpu.VMEM((n_kv, rb, LANES), F32), sq_in=pltpu.VMEM((n_kv, rb, LANES), F32),
-            sq_s=dma((n_kv,)), sq_r=dma((n_kv,)),
             p=pltpu.VMEM(swap, BF), q=pltpu.VMEM(swap, BF), o=pltpu.VMEM((n_tp, rt, width), BF),
-            ps=dma(swap[:1]), pr=dma(swap[:1]), os=dma((n_tp,)), ur=dma((n_tp,)))
+            **squares, **tp_sems)
+
+    cuts = chunks_of(hidden)
+    half_sems, half_sums = [signals(True, True) for _ in cuts], sums()
+
+    def half():
+        return phase([exchange(2, size, size, sems) for (_, size), sems in zip(cuts, half_sems)], half_sums)
 
     tree = dict(
         held={name: pltpu.VMEM(a.shape, a.dtype) for name, a in streamed.items()},
         load_sem=dma((len(streamed) + 2 * len(chunks_of(hidden)),)),
         scaled=pltpu.VMEM((rows, width), BF),
         acc=pltpu.VMEM((rows, width), F32),
-        first=phase([exchange(2, size, size) for _, size in chunks_of(hidden)]),
-        mix=phase([exchange(1, 2 * dm + LANES, dm), exchange(1, 2 * dm, 0)]),
-        second=phase([exchange(2, size, size) for _, size in chunks_of(hidden)]),
+        first=half(),
+        mix=phase([exchange(1, 2 * dm + LANES, dm, signals(False, True)),
+                   exchange(1, 2 * dm, 0, signals(False, False))], sums()),
+        second=half(),
         row_q=pltpu.VMEM((heads, rb, head_size), F32),
         row_k=pltpu.VMEM((heads, rb, head_size), F32),
         row_c=pltpu.VMEM((heads, rb, head_size), F32),
@@ -584,6 +623,9 @@
             return {key: number(value) for key, value in node.items()}
         if isinstance(node, list):
             return [number(value) for value in node]
+        for at, shape in enumerate(shapes):
+            if shape is node:
+                return at
         shapes.append(node)
         return len(shapes) - 1
 

time: 98.2 us -> 94.4 us (0.961)
  Pallas kernels: 97.4 us -> 93.6 us
    pallas_call x1, Pallas kernels: 93.7 us -> 89.9 us  [on_device(): pl.pallas_call(functools.partial(layer_kernel, n_kv, n_tp, unpack), out_s...]
where the time goes in v4:
time: 94.4 us; the launch traced here: 94.3 us
  Pallas kernels  93.6 us (99%)
    pallas_call x1, Pallas kernels, on_device(): pl.pallas_call(functools.partial(layer_kernel, n_kv, n_tp, unpack), out_s...  89.9 us
    pallas_call x1, Pallas kernels, on_device(): pl.pallas_call(functools.partial(results_kernel, count, len(passed)), out...  3.67 us

profile of v4, /device:TPU:0, one launch (start us, length us, event | category | flops | bytes accessed | tf_op | source)
XLA Modules:
  0.0 94.3 jit_solution(1874530043228703934)
XLA Ops:
  0.6 89.9 %shard_map.228 = (bf16[128,512]{1,0:T(8,128)(2,1)}, f32[16,4,128,128]{3,2,1,0:T(8,128)}, f32[16,4,128]{2,1,0:T(4,128)}, f32[4,16]{1,0:T(4,128)}) custom-call(f32[4]{0:T(128)} %refs_0_.1, bf16[128,512]{1,0:T(8,128)(2,1)} %refs_1_.1, f32[1,512]{1,0:T(1,128)} %bitcast.17, bf16[2752,512]{1,0:T(8,128)(2,1)} %bitcast.11, bf16[2752,512]{1,0:T(8,128)(2,1)} %bitcast.12, ...), custom_call_target="tpu_custom_call" | custom-call | tf_op jit(solution)/shard_map/pallas_call | solution.py:651
  90.6 3.7 %shard_map.229 = (f32[16,4,128,128]{3,2,1,0:T(8,128)}, bf16[128,512]{1,0:T(8,128)(2,1)}, f32[16,4,128]{2,1,0:T(4,128)}, f32[4,16]{1,0:T(4,128)}) custom-call(f32[16,4,128,128]{3,2,1,0:T(8,128)} %get-tuple-element.12.refs_0_, bf16[128,512]{1,0:T(8,128)(2,1)} %get-tuple-element.13.refs_1_, f32[16,4,128]{2,1,0:T(4,128)} %get-tuple-element.14.refs_2_, ...), custom_call_target="tpu_custom_call" | custom-call | tf_op jit(solution)/shard_map/pallas_call | solution.py:662
